TPU v7x, 32 devices: a whole 2x2x4 slice. The times are simulated.
32 devices in a mesh: ep: 16 (over z, x, core), tp: 2 (over y).
Axes of the slice: x: 2, y: 2, z: 4, core: 2. Of those that a mesh axis runs over, the one named last changes fastest.
Arguments:
- tokens: bfloat16 [2048, 2048], P('ep'), may hold values from -6 to 6
- routes: int32 [2048, 2], P('ep'), may hold values from 0 to 3, all different within a row; in each aligned block of 128 rows (0 to 127, 128 to 255, ...) at most 80 rows name the same one
- router_weight: bfloat16 [2048, 4], replicated, may hold values from -0.125 to 0.125
- gate_proj: bfloat16 [16, 2048, 1024], P('ep', None, 'tp'), may hold values from -0.125 to 0.125
- up_proj: bfloat16 [16, 2048, 1024], P('ep', None, 'tp'), may hold values from -0.125 to 0.125
- down_proj: bfloat16 [16, 1024, 2048], P('ep', 'tp'), may hold values from -0.09375 to 0.09375
- cotangent: bfloat16 [2048, 2048], P('ep'), may hold values from -1.5 to 1.5
Outputs:
- token_grad: bfloat16 [2048, 2048], P('ep', 'tp')
- gate_grad: float32 [2048, 2], P('ep')
- router_grad: float32 [2048, 4], P('ep')
- gate_proj_grad: float32 [16, 2048, 1024], P('ep', None, 'tp')
- up_proj_grad: float32 [16, 2048, 1024], P('ep', None, 'tp')
- down_proj_grad: float32 [16, 1024, 2048], P('ep', 'tp')
Inputs may be any that keep to these rules, and one draw needn't show every extreme that they name: `routes`: each row names 2 different experts. Among the rows of one index of ep no expert is named more than 80 times, a bound that some block reaches.
All inputs are finite; a program needn't handle non-finite values.
Results may differ from a plain program's by a relative error of at most 0.0085.
Values may be sent and summed in bfloat16 or wider, within the bound.
A program may use at most 128 MiB of HBM per device.

v0:
```python
import jax
import jax.numpy as jnp
from jax import lax
from jax.sharding import PartitionSpec as P

MEMBERS = 4
TOP = 2


def shards(tokens, routes, router_weight, gate_proj, up_proj, down_proj, cotangent):
    ntok = tokens.shape[0]
    width = tokens.shape[1]
    experts = router_weight.shape[1]
    n_ep = lax.axis_size("ep")
    n_tp = lax.axis_size("tp")
    share = width // n_tp
    capacity = min(ntok, 5 * TOP * ntok // (4 * experts))
    tp_index = lax.axis_index("tp")
    logits = jnp.dot(tokens, router_weight, preferred_element_type=jnp.float32)
    onehot = (routes[:, :, None] == jnp.arange(experts, dtype=jnp.int32)[None, None, :]).astype(
        jnp.float32
    )
    chosen = jnp.sum(onehot * logits[:, None, :], axis=2)
    first = jax.nn.sigmoid(chosen[:, 0] - chosen[:, 1])
    gates = jnp.stack([first, 1.0 - first], axis=1)
    used = gates.astype(jnp.bfloat16)
    flat = onehot.reshape(ntok * TOP, experts)
    rank = jnp.cumsum(flat, axis=0) - flat
    rank_sel = jnp.sum(flat * rank, axis=1).astype(jnp.int32)
    target = routes.reshape(-1) * capacity + rank_sel
    placing = (jnp.arange(experts * capacity, dtype=jnp.int32)[:, None] == target[None, :]).astype(
        jnp.float32
    )
    place_tok = jnp.sum(placing.reshape(experts * capacity, ntok, TOP), axis=2)
    place_bf = place_tok.astype(jnp.bfloat16)

    def spread(buffer):
        tail = buffer.shape[1:]
        grown = jnp.broadcast_to(
            buffer.reshape((experts, 1, capacity) + tail), (experts, MEMBERS, capacity) + tail
        )
        return grown.reshape((n_ep * capacity,) + tail)

    gate_slots = jnp.dot(
        placing, used.reshape(-1).astype(jnp.float32), precision=lax.Precision.HIGHEST
    ).astype(jnp.bfloat16)
    gate_send = spread(gate_slots[:, None])[:, 0]
    tok_part = lax.dynamic_slice_in_dim(tokens, tp_index * share, share, 1)
    cot_part = lax.dynamic_slice_in_dim(cotangent, tp_index * share, share, 1)
    tok_send = spread(
        jnp.dot(place_bf, tok_part, preferred_element_type=jnp.float32).astype(jnp.bfloat16)
    )
    cot_send = spread(
        jnp.dot(place_bf, cot_part, preferred_element_type=jnp.float32).astype(jnp.bfloat16)
    )
    tok_half, cot_half, gate_rows = (
        lax.all_to_all(tok_send, "ep", split_axis=0, concat_axis=0, tiled=True),
        lax.all_to_all(cot_send, "ep", split_axis=0, concat_axis=0, tiled=True),
        lax.all_to_all(gate_send, "ep", split_axis=0, concat_axis=0, tiled=True),
    )
    tok_rows, cot_rows = (
        lax.all_gather(tok_half, "tp", axis=1, tiled=True),
        lax.all_gather(cot_half, "tp", axis=1, tiled=True),
    )
    w_gate = gate_proj[0]
    w_up = up_proj[0]
    w_down = down_proj[0]
    gpre = jnp.dot(tok_rows, w_gate, preferred_element_type=jnp.float32)
    upre = jnp.dot(tok_rows, w_up, preferred_element_type=jnp.float32)
    sig = jax.nn.sigmoid(gpre)
    silu_val = gpre * sig
    hidden = (silu_val * upre).astype(jnp.bfloat16)
    qvals = lax.dot_general(
        cot_rows, w_down, (((1,), (1,)), ((), ())), preferred_element_type=jnp.float32
    )
    gate_part = jnp.sum(hidden.astype(jnp.float32) * qvals, axis=1)
    weight = gate_rows.astype(jnp.float32)[:, None]
    dhid = weight * qvals
    d_gate = (dhid * upre * sig * (1.0 + gpre * (1.0 - sig))).astype(jnp.bfloat16)
    d_up = (dhid * silu_val).astype(jnp.bfloat16)
    scaled = (weight * hidden.astype(jnp.float32)).astype(jnp.bfloat16)
    grad_down = lax.dot_general(
        scaled, cot_rows, (((0,), (0,)), ((), ())), preferred_element_type=jnp.float32
    )
    grad_gate = lax.dot_general(
        tok_rows, d_gate, (((0,), (0,)), ((), ())), preferred_element_type=jnp.float32
    )
    grad_up = lax.dot_general(
        tok_rows, d_up, (((0,), (0,)), ((), ())), preferred_element_type=jnp.float32
    )
    row_grad = lax.dot_general(
        d_gate, w_gate, (((1,), (1,)), ((), ())), preferred_element_type=jnp.float32
    )
    row_grad = row_grad + lax.dot_general(
        d_up, w_up, (((1,), (1,)), ((), ())), preferred_element_type=jnp.float32
    )
    row_share = lax.psum_scatter(row_grad, "tp", scatter_dimension=1, tiled=True)
    gate_total = lax.psum(gate_part, "tp")
    back_rows, back_gate = (
        lax.all_to_all(row_share, "ep", split_axis=0, concat_axis=0, tiled=True),
        lax.all_to_all(gate_total, "ep", split_axis=0, concat_axis=0, tiled=True),
    )
    back_rows = jnp.sum(back_rows.reshape(experts, MEMBERS, capacity, share), axis=1).reshape(
        experts * capacity, share
    )
    back_gate = jnp.sum(back_gate.reshape(experts, MEMBERS, capacity), axis=1).reshape(
        experts * capacity
    )
    route_sum = lax.dot_general(
        place_tok, back_rows, (((0,), (0,)), ((), ())), precision=lax.Precision.HIGHEST
    )
    gate_grad = lax.dot_general(
        placing, back_gate, (((0,), (0,)), ((), ())), precision=lax.Precision.HIGHEST
    ).reshape(ntok, TOP)
    delta = first * (1.0 - first) * (gate_grad[:, 0] - gate_grad[:, 1])
    dlogits = delta[:, None] * (onehot[:, 0] - onehot[:, 1])
    router_rows = lax.dynamic_slice_in_dim(router_weight, tp_index * share, share, 0).astype(
        jnp.float32
    )
    router_part = lax.dot_general(
        dlogits, router_rows, (((1,), (1,)), ((), ())), precision=lax.Precision.HIGHEST
    )
    token_grad = (route_sum + router_part).astype(jnp.bfloat16)
    columns = tokens.astype(jnp.float32)
    router_grad = lax.psum_scatter(
        lax.dot_general(
            columns, dlogits, (((0,), (0,)), ((), ())), precision=lax.Precision.HIGHEST
        ),
        "ep",
        scatter_dimension=0,
        tiled=True,
    )
    return (token_grad, gate_grad, router_grad, grad_gate[None], grad_up[None], grad_down[None])


def solution(mesh):
    placed = (
        P("ep", None),
        P("ep", None),
        P(),
        P("ep", None, "tp"),
        P("ep", None, "tp"),
        P("ep", "tp", None),
        P("ep", None),
    )
    return jax.shard_map(
        shards,
        mesh=mesh,
        in_specs=placed,
        out_specs=(
            P("ep", "tp"),
            P("ep", None),
            P("ep", None),
            P("ep", None, "tp"),
            P("ep", None, "tp"),
            P("ep", "tp", None),
        ),
        check_vma=False,
    )
```

profile of v0, /device:TPU:0, one launch (start us, length us, event | category | flops | bytes accessed | tf_op | source)
XLA Modules:
  0.0 487.1 jit_solution(1121042243303813282)
XLA Ops:
  8.5 1.2 reduce-window.6
  11.1 1.3 convolution_convert_fusion
  12.7 65.7 %all_to_all.51 = bf16[16,80,1024]{2,1,0:T(8,128)(2,1)} all-to-all(bf16[16,80,1024]{2,1,0:T(8,128)(2,1)S(1)} %bitcast.86), channel_id=1, replica_groups=mesh['ep'=16,'tp'=2] {'ep'}, dimensions={0} | all-to-all | bytes 5242880 | tf_op jit(solution)/shard_map/all_to_all | solution.py:57
  80.1 63.5 %all_to_all.52 = bf16[16,80,1024]{2,1,0:T(8,128)(2,1)} all-to-all(bf16[16,80,1024]{2,1,0:T(8,128)(2,1)S(1)} %bitcast.87), channel_id=1, replica_groups=mesh['ep'=16,'tp'=2] {'ep'}, dimensions={0} | all-to-all | bytes 5242880 | tf_op jit(solution)/shard_map/all_to_all | solution.py:58
  143.7 1.0 copy-done.2
  145.6 11.4 %all_to_all.53 = bf16[16,80,1]{1,2,0:T(2,128)(2,1)S(1)} all-to-all(bf16[16,80,1]{1,2,0:T(2,128)(2,1)S(1)} %copy.64), channel_id=1, replica_groups=mesh['ep'=16,'tp'=2] {'ep'}, dimensions={0} | all-to-all | bytes 5120 | tf_op jit(solution)/shard_map/all_to_all | solution.py:59
  157.1 7.8 %fusion.5 = f32[1280,512]{0,1:T(8,128)} fusion(bf16[1280,2048]{1,0:T(8,128)(2,1)} %all-gather.5.cloned.1.call-done, bf16[1,2048,512]{2,1,0:T(8,128)(2,1)S(1)} %copy-done), kind=kOutput, calls=%fused_computation.17 | convolution fusion | flops 2684354560 | bytes 9961472 | tf_op jit(solution)/shard_map/dot_general | solution.py:68
  164.9 4.6 fusion.8
  169.6 48.3 %all-gather.3.cloned.1.call-done = bf16[1280,2048]{1,0:T(8,128)(2,1)} async-done(((bf16[1280,1024]{1,0:T(8,128)(2,1)}), bf16[1280,2048]{1,0:T(8,128)(2,1)}) %all-gather.3.cloned.1.call-update) | async-done | bytes 5242896 | tf_op jit(solution)/shard_map/all_gather | solution.py:63
  217.8 9.6 %fusion = (f32[1280]{0:T(1024)S(1)}, bf16[1280,512]{0,1:T(8,128)(2,1)}, bf16[1280,512]{0,1:T(8,128)(2,1)S(1)}, bf16[1280,512]{0,1:T(8,128)(2,1)S(1)}) fusion(f32[1280,512]{0,1:T(8,128)} %fusion.8, f32[1280,512]{0,1:T(8,128)} %fusion.5, f32[1280]{0:T(1024)S(1)} %reshape.131, bf16[1280,2048]{1,0:T(8,128)(2,1)} %all-gather.3.cloned.1.call-done, ...), kind=kOutput, calls=%fused_computation.7 | convolution fusion | flops 2696805120 | bytes 16525312 | tf_op jit(solution)/shard_map/dot_general | solution.py:73
  227.5 3.2 fusion.3
  230.7 5.6 %convolution_add_fusion = f32[1280,2048]{1,0:T(8,128)} fusion(f32[1280,2048]{1,0:T(8,128)S(1)} %fusion.3, bf16[1280,512]{0,1:T(8,128)(2,1)S(1)} %get-tuple-element.11, bf16[1,2048,512]{2,1,0:T(8,128)(2,1)S(1)} %copy-done.7), kind=kOutput, calls=%fused_computation | convolution fusion | flops 2686976000 | bytes 24379392 | tf_op jit(solution)/shard_map/dot_general | solution.py:94
  236.4 5.0 %psum.7 = f32[16,80,1]{1,0,2:T(8,128)S(1)} all-reduce(f32[16,80,1]{1,0,2:T(8,128)S(1)} %all_to_all.44), channel_id=1, replica_groups=mesh['ep'=16,'tp'=2] {'tp'}, use_global_device_ids=true, to_apply=%region_8.9 | all-reduce | flops 1280 | bytes 10240 | tf_op jit(solution)/shard_map/psum | solution.py:98
  241.3 11.8 %all_to_all.54 = f32[16,80,1]{1,2,0:T(1,128)S(1)} all-to-all(f32[16,80,1]{1,2,0:T(1,128)S(1)} %bitcast.93), channel_id=1, replica_groups=mesh['ep'=16,'tp'=2] {'ep'}, dimensions={0} | all-to-all | bytes 10240 | tf_op jit(solution)/shard_map/all_to_all | solution.py:101
  253.2 105.2 %reduce-scatter.5.cloned.1.call-done = f32[1280,1024]{1,0:T(8,128)} async-done(((f32[1280,2048]{1,0:T(8,128)}), f32[1280,1024]{1,0:T(8,128)}) %reduce-scatter.5.cloned.1.call-update) | async-done | bytes 5242896 | tf_op jit(solution)/shard_map/reduce_scatter | solution.py:97
  358.4 5.8 %all-to-all-start.3 = ((f32[16,80,1024]{2,1,0:T(8,128)}), f32[16,80,1024]{2,1,0:T(8,128)}, u32[]{:S(2)}, u32[]{:S(2)}) async-start(f32[16,80,1024]{2,1,0:T(8,128)} %bitcast.88), calls=%async_computation.4 | async-start | bytes 10485760 | tf_op jit(solution)/shard_map/all_to_all | solution.py:100
  364.5 7.2 %convolution_bitcast_fusion.2 = f32[1,2048,512]{2,1,0:T(8,128)} fusion(bf16[1280,2048]{1,0:T(8,128)(2,1)} %all-gather.5.cloned.1.call-done, bf16[1280,512]{0,1:T(8,128)(2,1)S(1)} %copy-done.14), kind=kOutput, calls=%fused_computation.6 | convolution fusion | flops 2684354560 | bytes 10747904 | tf_op jit(solution)/shard_map/dot_general | solution.py:85
  371.8 7.2 %convolution_bitcast_fusion.1 = f32[1,2048,512]{2,1,0:T(8,128)} fusion(bf16[1280,2048]{1,0:T(8,128)(2,1)} %all-gather.5.cloned.1.call-done, bf16[1280,512]{0,1:T(8,128)(2,1)S(1)} %get-tuple-element.11), kind=kOutput, calls=%fused_computation.5 | convolution fusion | flops 2684354560 | bytes 10747904 | tf_op jit(solution)/shard_map/dot_general | solution.py:88
  379.0 4.5 convolution_bitcast_fusion
  384.4 1.4 copy.71
  386.2 87.7 %reduce-scatter.7.cloned.1.call-done = f32[128,4]{1,0:T(8,128)} async-done(((f32[2048,4]{1,0:T(8,128)}), f32[128,4]{1,0:T(8,128)}) %reduce-scatter.7.cloned.1.call-update) | async-done | bytes 2064
  473.9 1.5 copy.72
  475.4 3.3 bitcast_reduce_fusion
  478.8 1.8 fusion.14
  (90 shorter events, 7.4 us)
Async XLA Ops:
  7.2 150.0 %copy-start = (bf16[1,2048,512]{2,1,0:T(8,128)(2,1)S(1)}, bf16[1,2048,512]{2,1,0:T(8,128)(2,1)}, u32[]{:S(2)}) copy-start(bf16[1,2048,512]{2,1,0:T(8,128)(2,1)} %param.10) | copy-start | bytes 6291460
  7.2 149.9 %all-gather.5.cloned.1.call-start = ((), (), s32[]{:S(2)}) async-start(), calls=%async_computation.8 | async-start | bytes 7864320 | tf_op jit(solution)/shard_map/all_gather | solution.py:62
  11.1 67.4 %copy-start.4 = (f32[320,128]{1,0:T(8,128)}, f32[320,128]{1,0:T(8,128)S(1)}, u32[]{:S(2)}) copy-start(f32[320,128]{1,0:T(8,128)S(1)} %convert_reduce_fusion) | copy-start | bytes 491524
  78.4 1.0 copy-start.8
  78.5 139.4 %all-gather.3.cloned.1.call-start = ((), (), s32[]{:S(2)}) async-start(), calls=%async_computation.7 | async-start | bytes 7864320 | tf_op jit(solution)/shard_map/all_gather | solution.py:63
  143.6 1.0 copy-start.2
  143.6 1.0 copy-start.9
  143.6 1.3 copy-start.10
  143.6 214.7 %reduce-scatter.5.cloned.1.call-start = ((), (), s32[]{:S(2)}) async-start(), calls=%async_computation.9 | async-start | bytes 15728640 | tf_op jit(solution)/shard_map/reduce_scatter | solution.py:97
  157.1 7.8 %copy-start.6 = (bf16[1,2048,512]{2,1,0:T(8,128)(2,1)S(1)}, bf16[1,2048,512]{2,1,0:T(8,128)(2,1)}, u32[]{:S(2)}) copy-start(bf16[1,2048,512]{2,1,0:T(8,128)(2,1)} %param.11) | copy-start | bytes 6291460
  157.1 7.8 %copy-start.12 = (bf16[1280,2048]{1,0:T(8,128)(2,1)S(1)}, bf16[1280,2048]{1,0:T(8,128)(2,1)}, u32[]{:S(2)}) copy-start(bf16[1280,2048]{1,0:T(8,128)(2,1)} %all-gather.5.cloned.1.call-done) | copy-start | bytes 15728644
  227.5 3.2 copy-start.13
  227.5 3.2 copy-start.7
  358.4 6.1 %copy-start.14 = (bf16[1280,512]{0,1:T(8,128)(2,1)S(1)}, bf16[1280,512]{0,1:T(8,128)(2,1)}, u32[]{:S(2)}) copy-start(bf16[1280,512]{0,1:T(8,128)(2,1)} %copy-done.13) | copy-start | bytes 3932164
  358.4 117.0 %all-to-all-start.3 = ((f32[16,80,1024]{2,1,0:T(8,128)}), f32[16,80,1024]{2,1,0:T(8,128)}, u32[]{:S(2)}, u32[]{:S(2)}) async-start(f32[16,80,1024]{2,1,0:T(8,128)} %bitcast.88), calls=%async_computation.4 | async-start | bytes 10485760 | tf_op jit(solution)/shard_map/all_to_all | solution.py:100
  364.2 109.7 %reduce-scatter.7.cloned.1.call-start = ((), (), s32[]{:S(2)}) async-start(), calls=%async_computation.10 | async-start | bytes 1114112
  364.5 14.5 %slice-start = ((s8[5242880]{0:T(1024)(128)(4,1)}), s8[4194304]{0:T(1024)(128)(4,1)S(1)}, s32[]{:S(2)}) async-start(s8[5242880]{0:T(1024)(128)(4,1)} %bitcast.96), calls=%async_computation.11 | async-start | bytes 8388608
  371.8 7.2 %slice-start.1 = ((s8[5242880]{0:T(1024)(128)(4,1)}), s8[1048576]{0:T(1024)(128)(4,1)S(1)}, s32[]{:S(2)}) async-start(s8[5242880]{0:T(1024)(128)(4,1)} %bitcast.96), calls=%async_computation.12 | async-start | bytes 2097152
  371.8 7.2 %copy-start.15 = (bf16[1280,512]{0,1:T(8,128)(2,1)S(1)}, bf16[1280,512]{0,1:T(8,128)(2,1)}, u32[]{:S(2)}) copy-start(bf16[1280,512]{0,1:T(8,128)(2,1)} %get-tuple-element.9) | copy-start | bytes 3932164
  379.0 5.0 %copy-start.3 = (bf16[128,2048]{1,0:T(8,128)(2,1)S(1)}, bf16[128,2048]{1,0:T(8,128)(2,1)}, u32[]{:S(2)}) copy-start(bf16[128,2048]{1,0:T(8,128)(2,1)} %param.7) | copy-start | bytes 1572868
  384.0 94.7 %copy-start.11 = (f32[128,2]{0,1:T(2,128)}, f32[128,2]{0,1:T(2,128)S(1)}, u32[]{:S(2)}) copy-start(f32[128,2]{0,1:T(2,128)S(1)} %copy.70) | copy-start | bytes 3076
  475.4 3.4 copy-start.5
  475.4 5.2 %copy-start.1 = (bf16[1,2048,512]{2,1,0:T(8,128)(2,1)S(1)}, bf16[1,2048,512]{2,1,0:T(8,128)(2,1)}, u32[]{:S(2)}) copy-start(bf16[1,2048,512]{2,1,0:T(8,128)(2,1)} %param.10) | copy-start | bytes 6291460
Sparse Core Ops, SparseCore 0:
  78.6 69.0 all-gather.4
  149.3 68.5 all-gather.2
  236.4 121.9 reduce-scatter.4
  385.9 87.9 reduce-scatter.6
where the time goes:
time: 497 us; the launch traced here: 487 us
  waiting for transfers between devices  241 us (48%)
  blocking collectives  157 us (32%)
  matrix products  54.3 us (11%)
  between operations  14.1 us (3%)
  local copies, waits for them, and re-layouts  8.03 us (2%)
  other arithmetic  6.06 us (1%)
  starting transfers between devices  5.97 us (1%)
    reduce_scatter x1, waiting for transfers between devices, shards(): lax.psum_scatter(row_grad, 'tp', scatter_dimension=1, tiled=True)  105 us
    unnamed x5, waiting for transfers between devices  87.7 us
    all_to_all x1, blocking collectives, shards(): lax.all_to_all(tok_send, 'ep', split_axis=0, concat_axis=0, tiled=True)  65.7 us
    all_to_all x1, blocking collectives, shards(): lax.all_to_all(cot_send, 'ep', split_axis=0, concat_axis=0, tiled=True)  63.5 us
    all_gather x1, waiting for transfers between devices, shards(): lax.all_gather(cot_half, 'tp', axis=1, tiled=True)  48.3 us
    all_to_all x1, blocking collectives, shards(): lax.all_to_all(gate_total, 'ep', split_axis=0, concat_axis=0, tiled=True)  11.8 us
    all_to_all x1, blocking collectives, shards(): lax.all_to_all(gate_send, 'ep', split_axis=0, concat_axis=0, tiled=True)  11.4 us
  transfers between devices with their start and end apart: 5, of which 3 were waited for; matrix products, arithmetic and copies ran while one was open for 8% of the time, Pallas kernels for 0%

commit v1 on v0

v1 whole, which is shorter than its diff:
```python
import functools

import jax
import jax.numpy as jnp
from jax import lax
from jax.experimental import pallas as pl
from jax.experimental.pallas import tpu as pltpu
from jax.sharding import Mesh, PartitionSpec as P

MEMBERS = 4
TOP = 2
LANES = 128
F32 = jnp.float32
BF16 = jnp.bfloat16
NT = (((1,), (1,)), ((), ()))


def rows_kernel(share, x_ref, wg_ref, wu_ref, wd_ref, dg_ref, du_ref, sc_ref, back_ref):
    n_tp = x_ref.shape[1]
    experts = lax.axis_size("e")
    e_idx = lax.axis_index("e")

    def contract(base, w_ref, dims):
        total = None
        for t in range(n_tp):
            part = x_ref[0, t, :, base : base + share]
            if dims is None:
                term = jnp.dot(part, w_ref[0, t * share : (t + 1) * share, :], preferred_element_type=F32)
            else:
                term = lax.dot_general(
                    part, w_ref[0, :, t * share : (t + 1) * share], dims, preferred_element_type=F32
                )
            total = term if total is None else total + term
        return total

    gpre = contract(0, wg_ref, None)
    upre = contract(0, wu_ref, None)
    qvals = contract(share, wd_ref, NT)
    extra = x_ref[0, 0, :, 2 * share :].astype(F32)
    lane = lax.broadcasted_iota(jnp.int32, extra.shape, 1)
    weight = jnp.sum(jnp.where(lane == experts + e_idx, extra, 0.0), axis=1, keepdims=True)
    sig = jax.nn.sigmoid(gpre)
    silu_val = gpre * sig
    hidden = (silu_val * upre).astype(BF16).astype(F32)
    gate_part = jnp.sum(hidden * qvals, axis=1, keepdims=True)
    dhid = weight * qvals
    d_gate = (dhid * upre * sig * (1.0 + gpre * (1.0 - sig))).astype(BF16)
    d_up = (dhid * silu_val).astype(BF16)
    dg_ref[0] = d_gate
    du_ref[0] = d_up
    sc_ref[0] = (weight * hidden).astype(BF16)
    gate_lanes = jnp.where(lane == e_idx, gate_part, 0.0).astype(BF16)
    for t in range(n_tp):
        cols = slice(t * share, (t + 1) * share)
        grad = lax.dot_general(d_gate, wg_ref[0, cols, :], NT, preferred_element_type=F32)
        grad = grad + lax.dot_general(d_up, wu_ref[0, cols, :], NT, preferred_element_type=F32)
        back_ref[0, t, :, :share] = grad.astype(BF16)
        back_ref[0, t, :, share:] = gate_lanes


def grads_kernel(x_ref, c_ref, dg_ref, du_ref, sc_ref, gg_ref, gu_ref, gd_ref, sct):
    @pl.when(pl.program_id(0) == 0)
    def _():
        sct[...] = sc_ref[...].T

    tile = x_ref.shape[-1]
    rows = dg_ref.shape[0]
    xt = x_ref[:, 0].reshape(rows, tile).T
    gg_ref[0] = jnp.dot(xt, dg_ref[...], preferred_element_type=F32)
    gu_ref[0] = jnp.dot(xt, du_ref[...], preferred_element_type=F32)
    gd_ref[0] = jnp.dot(sct[...], c_ref[:, 0].reshape(rows, tile), preferred_element_type=F32)


def shards(tokens, routes, router_weight, gate_proj, up_proj, down_proj, cotangent):
    ntok, width = tokens.shape
    experts = router_weight.shape[1]
    n_m, n_tp = lax.axis_size("m"), lax.axis_size("tp")
    share = width // n_tp
    capacity = min(ntok, 5 * TOP * ntok // (4 * experts))
    tp_index = lax.axis_index("tp")
    e_index = lax.axis_index("e")
    ff = gate_proj.shape[2]

    logits = jnp.dot(tokens, router_weight, preferred_element_type=F32)
    onehot = (routes[:, :, None] == jnp.arange(experts, dtype=jnp.int32)[None, None, :]).astype(F32)
    chosen = jnp.sum(onehot * logits[:, None, :], axis=2)
    first = jax.nn.sigmoid(chosen[:, 0] - chosen[:, 1])
    gates = jnp.stack([first, 1.0 - first], axis=1)
    used = gates.astype(BF16)
    named = jnp.sum(onehot, axis=1)
    below = (jnp.arange(ntok)[:, None] > jnp.arange(ntok)[None, :]).astype(BF16)
    rank = jnp.dot(below, named.astype(BF16), preferred_element_type=F32)
    slot_cols = jnp.where(named > 0, rank, 255.0).astype(BF16)
    gate_cols = jnp.sum(onehot * used.astype(F32)[:, :, None], axis=1).astype(BF16)
    extras = jnp.concatenate(
        [slot_cols, gate_cols, jnp.zeros((ntok, LANES - 2 * experts), BF16)], axis=1
    )
    send = jnp.concatenate(
        [
            lax.dynamic_slice_in_dim(tokens, tp_index * share, share, 1),
            lax.dynamic_slice_in_dim(cotangent, tp_index * share, share, 1),
            extras,
        ],
        axis=1,
    )
    near = lax.all_gather(send, "e", axis=0, tiled=False)
    lanes = jnp.arange(LANES)[None, None, :]
    slot = jnp.sum(jnp.where(lanes == e_index, near[:, :, 2 * share :].astype(F32), 0.0), axis=2)
    place = (
        jnp.arange(capacity, dtype=jnp.int32)[None, :, None] == slot.astype(jnp.int32)[:, None, :]
    ).astype(BF16)
    rows = jnp.einsum("ect,etw->ecw", place, near, preferred_element_type=F32).astype(BF16)
    held = experts * capacity
    wide = 2 * share + LANES
    full = lax.all_gather(rows.reshape(held, wide), ("m", "tp"), axis=0, tiled=False)
    full = full.reshape(n_m, n_tp, held, wide)

    back_wide = share + LANES
    hid_spec = pl.BlockSpec((1, held, ff), lambda i: (i, 0, 0))
    hid_shape = jax.ShapeDtypeStruct((n_m, held, ff), BF16)
    flops = 2 * n_m * held * width * ff
    d_gate, d_up, scaled, back = pl.pallas_call(
        functools.partial(rows_kernel, share),
        grid=(n_m,),
        in_specs=[
            pl.BlockSpec((1, n_tp, held, wide), lambda i: (i, 0, 0, 0)),
            pl.BlockSpec((1, width, ff), lambda i: (0, 0, 0)),
            pl.BlockSpec((1, width, ff), lambda i: (0, 0, 0)),
            pl.BlockSpec((1, ff, width), lambda i: (0, 0, 0)),
        ],
        out_specs=[
            hid_spec,
            hid_spec,
            hid_spec,
            pl.BlockSpec((1, n_tp, held, back_wide), lambda i: (i, 0, 0, 0)),
        ],
        out_shape=[
            hid_shape,
            hid_shape,
            hid_shape,
            jax.ShapeDtypeStruct((n_m, n_tp, held, back_wide), BF16),
        ],
        cost_estimate=pl.CostEstimate(flops=5 * flops, bytes_accessed=30 << 20, transcendentals=0),
        name="rows",
    )(full, gate_proj, up_proj, down_proj)

    mine = lax.psum_scatter(
        back.reshape(n_m * n_tp, held, back_wide), ("m", "tp"), scatter_dimension=0, tiled=False
    )

    tile = 256
    per = share // tile
    total = n_m * held
    whole = lambda i: (0, 0)
    grad_gate, grad_up, grad_down = pl.pallas_call(
        grads_kernel,
        grid=(width // tile,),
        in_specs=[
            pl.BlockSpec((n_m, 1, held, tile), lambda i: (0, i // per, 0, i % per)),
            pl.BlockSpec((n_m, 1, held, tile), lambda i: (0, i // per, 0, per + i % per)),
            pl.BlockSpec((total, ff), whole),
            pl.BlockSpec((total, ff), whole),
            pl.BlockSpec((total, ff), whole),
        ],
        out_specs=[
            pl.BlockSpec((1, tile, ff), lambda i: (0, i, 0)),
            pl.BlockSpec((1, tile, ff), lambda i: (0, i, 0)),
            pl.BlockSpec((1, ff, tile), lambda i: (0, 0, i)),
        ],
        out_shape=[
            jax.ShapeDtypeStruct(gate_proj.shape, F32),
            jax.ShapeDtypeStruct(up_proj.shape, F32),
            jax.ShapeDtypeStruct(down_proj.shape, F32),
        ],
        scratch_shapes=[pltpu.VMEM((ff, total), BF16)],
        cost_estimate=pl.CostEstimate(flops=3 * flops, bytes_accessed=30 << 20, transcendentals=0),
        name="grads",
    )(full, full, d_gate.reshape(total, ff), d_up.reshape(total, ff), scaled.reshape(total, ff))

    dense = jnp.einsum(
        "ect,ecw->etw",
        place,
        mine.reshape(experts, capacity, back_wide),
        preferred_element_type=F32,
    ).astype(BF16)
    home = lax.psum_scatter(dense, "e", scatter_dimension=0, tiled=False).astype(F32)
    route_sum = home[:, :share]
    gate_grad = jnp.sum(onehot * home[:, None, share : share + experts], axis=2)
    delta = first * (1.0 - first) * (gate_grad[:, 0] - gate_grad[:, 1])
    dlogits = delta[:, None] * (onehot[:, 0] - onehot[:, 1])
    router_rows = lax.dynamic_slice_in_dim(router_weight, tp_index * share, share, 0).astype(F32)
    router_part = lax.dot_general(dlogits, router_rows, NT, precision=lax.Precision.HIGHEST)
    token_grad = (route_sum + router_part).astype(BF16)
    n_ep = lax.axis_size("e") * n_m
    terms = lax.dot_general(
        dlogits, tokens.astype(F32), (((0,), (0,)), ((), ())), precision=lax.Precision.HIGHEST
    )
    terms = terms.reshape(experts, n_ep, width // n_ep).transpose(1, 0, 2)
    terms = lax.all_to_all(terms, ("e", "m"), split_axis=0, concat_axis=0, tiled=True)
    router_grad = jnp.sum(terms, axis=0).T
    return (token_grad, gate_grad, router_grad, grad_gate, grad_up, grad_down)


def solution(mesh):
    devices = mesh.devices
    grid = Mesh(
        devices.reshape(devices.shape[0] // MEMBERS, MEMBERS, devices.shape[1]), ("e", "m", "tp")
    )
    ep = ("e", "m")
    return jax.shard_map(
        shards,
        mesh=grid,
        in_specs=(
            P(ep, None),
            P(ep, None),
            P(),
            P(ep, None, "tp"),
            P(ep, None, "tp"),
            P(ep, "tp", None),
            P(ep, None),
        ),
        out_specs=(
            P(ep, "tp"),
            P(ep, None),
            P(ep, None),
            P(ep, None, "tp"),
            P(ep, None, "tp"),
            P(ep, "tp", None),
        ),
        check_vma=False,
    )
```

time: 497 us -> 265 us (0.53); the launches traced: 487 us -> 265 us
  blocking collectives: 157 us -> 0 us
  waiting for transfers between devices: 241 us -> 195 us
  matrix products: 54.3 us -> 9.57 us
  Pallas kernels: 0 us -> 34.9 us
    all_to_all x4 -> x0, blocking collectives: 152 us -> none  [the longest x1 65.7 us: shards(): lax.all_to_all(tok_send, 'ep', split_axis=0, concat_axis=0, tiled=True)]
    unnamed x5 -> x4, waiting for transfers between devices: 87.7 us -> 0.07 us
    all_gather x2, waiting for transfers between devices: 48.3 us -> 115 us  [the longest x1 64.8 us: shards(): lax.all_gather(rows.reshape(held, wide), ('m', 'tp'), axis=0, tiled=False)]
    dot_general x15 -> x6, matrix products: 54.3 us -> 9.57 us  [the longest x1 3.24 us: shards(): jnp.einsum('ect,etw->ecw', place, near, preferred_element_type=F32)]
    pallas_call x0 -> x2, Pallas kernels: none -> 34.9 us  [the longest x1 20.2 us: shards(): pl.pallas_call(functools.partial(rows_kernel, share), grid=(n_m,), in_spe...]
    reduce_scatter x1 -> x2, waiting for transfers between devices: 105 us -> 74.2 us  [the longest x1 59.7 us: shards(): lax.psum_scatter(back.reshape(n_m * n_tp, held, back_wide), ('m', 'tp'),...]
    all_to_all x1, waiting for transfers between devices: 0.01 us -> 5.45 us  [shards(): lax.all_to_all(terms, ('e', 'm'), split_axis=0, concat_axis=0, tiled=True)]
    unnamed x39 -> x8, local copies, waits for them, and re-layouts: 5.81 us -> 0.68 us
  transfers between devices with their start and end apart: 5 -> 5, of which waited for: 3 -> 5; matrix products, arithmetic and copies ran while one was open for 8% -> 1% of each run, Pallas kernels for 0% -> 6%
where the time goes in v1:
time: 265 us
  waiting for transfers between devices  195 us (74%)
  Pallas kernels  34.9 us (13%)
  between operations  13.9 us (5%)
  matrix products  9.57 us (4%)
  other arithmetic  4.12 us (2%)
  starting transfers between devices  3.66 us (1%)
  local copies, waits for them, and re-layouts  3.34 us (1%)
    all_gather x1, waiting for transfers between devices, shards(): lax.all_gather(rows.reshape(held, wide), ('m', 'tp'), axis=0, tiled=False)  64.8 us
    reduce_scatter x1, waiting for transfers between devices, shards(): lax.psum_scatter(back.reshape(n_m * n_tp, held, back_wide), ('m', 'tp'),...  59.7 us
    all_gather x1, waiting for transfers between devices, shards(): near = lax.all_gather(send, 'e', axis=0, tiled=False)  50.6 us
    pallas_call x1, Pallas kernels, shards(): pl.pallas_call(functools.partial(rows_kernel, share), grid=(n_m,), in_spe...  20.2 us
    pallas_call x1, Pallas kernels, shards(): pl.pallas_call(grads_kernel, grid=(width // tile,), in_specs=[pl.BlockSpe...  14.7 us
    reduce_scatter x1, waiting for transfers between devices, shards(): lax.psum_scatter(dense, 'e', scatter_dimension=0, tiled=False).astype(F32)  14.5 us
    all_to_all x1, waiting for transfers between devices, shards(): lax.all_to_all(terms, ('e', 'm'), split_axis=0, concat_axis=0, tiled=True)  5.45 us
  transfers between devices with their start and end apart: 5, of which 5 were waited for; matrix products, arithmetic and copies ran while one was open for 1% of the time, Pallas kernels for 6%

profile of v1, /device:TPU:0, one launch (start us, length us, event | category | flops | bytes accessed | tf_op | source)
XLA Modules:
  0.0 264.6 jit_solution(1942644216735073602)
XLA Ops:
  7.2 0.7 copy-done
  7.9 1.3 fusion.16
  9.2 0.7 select_reduce_fusion.3
  9.9 0.7 select_reduce_fusion.2
  10.8 0.1 copy.16
  10.9 0.1 copy.17
  11.0 1.1 constant_dynamic-slice_fusion
  12.1 1.0 concatenate.8
  13.2 50.6 %all-gather.6.cloned.1.call-done = bf16[512,2176]{1,0:T(8,128)(2,1)} async-done(((bf16[128,2176]{1,0:T(8,128)(2,1)}), bf16[512,2176]{1,0:T(8,128)(2,1)}) %all-gather.6.cloned.1.call-update) | async-done | bytes 2228240 | tf_op jit(solution)/shard_map/all_gather | solution.py:106
  63.8 1.0 select_reduce_fusion
  64.8 3.2 %convolution_convert_fusion = bf16[4,80,2176]{2,1,0:T(8,128)(2,1)} fusion(bf16[4,128,2176]{2,1,0:T(8,128)(2,1)} %bitcast.34, s32[4,128]{1,0:T(4,128)S(1)} %convert_element_type.59), kind=kOutput, calls=%fused_computation | convolution fusion | flops 178995200 | bytes 3622912 | tf_op jit(solution)/shard_map/ect,etw->ecw/dot_general | solution.py:112
  68.2 64.8 %all-gather.4.cloned.1.call-done = bf16[8,320,2176]{2,1,0:T(8,128)(2,1)} async-done(((bf16[1,320,2176]{2,1,0:T(8,128)(2,1)}), bf16[8,320,2176]{2,1,0:T(8,128)(2,1)}) %all-gather.4.cloned.1.call-update) | async-done | bytes 11141136 | tf_op jit(solution)/shard_map/all_gather | solution.py:115
  132.9 20.2 %rows.1 = (bf16[4,320,512]{2,1,0:T(8,128)(2,1)}, bf16[4,320,512]{2,1,0:T(8,128)(2,1)}, bf16[4,320,512]{2,1,0:T(8,128)(2,1)}, bf16[4,2,320,1152]{3,2,1,0:T(8,128)(2,1)}) custom-call(bf16[4,2,320,2176]{3,2,1,0:T(8,128)(2,1)} %bitcast.38, bf16[1,2048,512]{2,1,0:T(8,128)(2,1)} %wg_ref.1, bf16[1,2048,512]{2,1,0:T(8,128)(2,1)} %wu_ref.1, bf16[1,512,2048]{2,1,0:T(8,128)(2,1)} %wd_ref.1), custom_call_target="tpu_custom_call" | custom-call | flops 13421772800 | bytes 31457280 | tf_op jit(solution)/shard_map/rows/pallas_call | solution.py:122
  153.2 59.7 %reduce-scatter.3.cloned.1.call-done = bf16[1,320,1152]{2,1,0:T(8,128)(2,1)} async-done(((bf16[8,320,1152]{2,1,0:T(8,128)(2,1)}), bf16[1,320,1152]{2,1,0:T(8,128)(2,1)}) %reduce-scatter.3.cloned.1.call-update) | async-done | bytes 737296 | tf_op jit(solution)/shard_map/reduce_scatter | solution.py:147
  212.9 2.6 %convolution_convert_fusion.1 = bf16[4,128,1152]{2,1,0:T(8,128)(2,1)} fusion(bf16[4,80,1152]{2,1,0:T(8,128)(2,1)} %bitcast.36, s32[4,128]{1,0:T(4,128)S(1)} %convert_element_type.59), kind=kOutput, calls=%fused_computation.1 | convolution fusion | flops 95002624 | bytes 1918976 | tf_op jit(solution)/shard_map/ect,ecw->etw/dot_general | solution.py:180
  215.6 0.3 copy.20
  215.9 14.7 %grads.1 = (f32[1,2048,512]{2,1,0:T(8,128)}, f32[1,2048,512]{2,1,0:T(8,128)}, f32[1,512,2048]{2,1,0:T(8,128)}) custom-call(bf16[4,2,320,2176]{3,2,1,0:T(8,128)(2,1)} %bitcast.39, bf16[4,2,320,2176]{3,2,1,0:T(8,128)(2,1)} %bitcast.40, bf16[1280,512]{1,0:T(8,128)(2,1)} %bitcast.41, bf16[1280,512]{1,0:T(8,128)(2,1)} %bitcast.42, bf16[1280,512]{1,0:T(8,128)(2,1)} %bitcast.43), custom_call_target="tpu_custom_call" | custom-call | flops 8053063680 | bytes 31457280 | tf_op jit(solution)/shard_map/grads/pallas_call | solution.py:155
  230.6 14.5 %reduce-scatter.5.cloned.1.call-done = bf16[1,128,1152]{2,1,0:T(8,128)(2,1)} async-done(((bf16[4,128,1152]{2,1,0:T(8,128)(2,1)}), bf16[1,128,1152]{2,1,0:T(8,128)(2,1)}) %reduce-scatter.5.cloned.1.call-update) | async-done | bytes 294928 | tf_op jit(solution)/shard_map/reduce_scatter | solution.py:186
  245.1 1.0 bitcast_convert_fusion
  246.2 1.1 convolution_bitcast_fusion
  247.3 3.5 %all-to-all-start = ((f32[16,4,128]{2,1,0:T(4,128)}), f32[16,4,128]{2,1,0:T(4,128)S(1)}, u32[]{:S(2)}, u32[]{:S(2)}) async-start(f32[16,4,128]{2,1,0:T(4,128)} %convolution_bitcast_fusion), calls=%async_computation.2 | async-start | bytes 65536 | tf_op jit(solution)/shard_map/all_to_all | solution.py:199
  250.8 1.1 fusion
  252.0 5.4 %all-to-all-done = f32[16,4,128]{2,1,0:T(4,128)S(1)} async-done(((f32[16,4,128]{2,1,0:T(4,128)}), f32[16,4,128]{2,1,0:T(4,128)S(1)}, u32[]{:S(2)}, u32[]{:S(2)}) %all-to-all-start) | async-done | bytes 32800 | tf_op jit(solution)/shard_map/all_to_all | solution.py:199
  257.4 0.6 reduce_sum.59
  (27 shorter events, 0.5 us)
Async XLA Ops:
  7.2 0.7 copy-start
  7.2 56.6 %all-gather.6.cloned.1.call-start = ((), (), s32[]{:S(2)}) async-start(), calls=%async_computation.6 | async-start | bytes 2785280 | tf_op jit(solution)/shard_map/all_gather | solution.py:106
  13.1 119.8 %all-gather.4.cloned.1.call-start = ((), (), s32[]{:S(2)}) async-start(), calls=%async_computation.3 | async-start | bytes 12533760 | tf_op jit(solution)/shard_map/all_gather | solution.py:115
  68.1 144.8 %reduce-scatter.3.cloned.1.call-start = ((), (), s32[]{:S(2)}) async-start(), calls=%async_computation.4 | async-start | bytes 6635520 | tf_op jit(solution)/shard_map/reduce_scatter | solution.py:147
  153.1 62.5 %copy-start.1 = (bf16[128,2048]{1,0:T(8,128)(2,1)S(1)}, bf16[128,2048]{1,0:T(8,128)(2,1)}, u32[]{:S(2)}) copy-start(bf16[128,2048]{1,0:T(8,128)(2,1)} %param.7) | copy-start | bytes 1572868
  153.2 62.7 %copy-start.2 = (s32[128,2]{0,1:T(2,128)S(1)}, s32[128,2]{0,1:T(2,128)}, u32[]{:S(2)}) copy-start(s32[128,2]{0,1:T(2,128)} %param.8) | copy-start | bytes 3076
  153.2 91.9 %reduce-scatter.5.cloned.1.call-start = ((), (), s32[]{:S(2)}) async-start(), calls=%async_computation.5 | async-start | bytes 1474560 | tf_op jit(solution)/shard_map/reduce_scatter | solution.py:186
  246.2 11.9 %copy-start.3 = (f32[128,2]{0,1:T(2,128)}, f32[128,2]{0,1:T(2,128)S(1)}, u32[]{:S(2)}) copy-start(f32[128,2]{0,1:T(2,128)S(1)} %select_reduce_fusion.1) | copy-start | bytes 3076
  247.3 10.1 %all-to-all-start = ((f32[16,4,128]{2,1,0:T(4,128)}), f32[16,4,128]{2,1,0:T(4,128)S(1)}, u32[]{:S(2)}, u32[]{:S(2)}) async-start(f32[16,4,128]{2,1,0:T(4,128)} %convolution_bitcast_fusion), calls=%async_computation.2 | async-start | bytes 65536 | tf_op jit(solution)/shard_map/all_to_all | solution.py:199
Sparse Core Ops, SparseCore 0:
  13.2 50.5 all-gather.5
  68.2 64.6 all-gather.3
  153.3 59.6 reduce-scatter.2
  215.7 29.3 reduce-scatter.4

commit v2 on v1

v2 whole, which is shorter than its diff:
```python
import functools

import jax
import jax.numpy as jnp
from jax import lax
from jax.experimental import pallas as pl
from jax.experimental.pallas import tpu as pltpu
from jax.sharding import Mesh, PartitionSpec as P

MEMBERS = 4
TOP = 2
LANES = 128
F32 = jnp.float32
BF16 = jnp.bfloat16
MESH = pl.DeviceIdType.MESH
NT = (((1,), (1,)), ((), ()))


def rows_kernel(
    share, send_ref, wg_hbm, wu_hbm, wd_hbm, x_hbm, dg_ref, du_ref, sc_ref, back_ref,
    full, wg_ref, wu_ref, wd_ref, out_sem, send_sem, recv_sem, load_sem,
):
    experts, n_m, n_tp, capacity, _ = full.shape
    e, m, t = lax.axis_index("e"), lax.axis_index("m"), lax.axis_index("tp")
    x_peer = lax.rem(m + 2, 4)
    core_peer = m + 1 - 2 * lax.rem(m, 2)
    held = n_m * capacity
    first_cols, last_cols = pl.ds(0, share), pl.ds(share, share + LANES)

    def ahead(j):
        return lax.rem(t + j, n_tp)

    def behind(j):
        return lax.rem(t + n_tp - j, n_tp)

    barrier = pltpu.get_barrier_semaphore()
    peers = [(lax.rem(e + k, experts), m, t) for k in range(1, experts)]
    peers += [(e, x_peer, t), (e, core_peer, t)] + [(e, m, ahead(j)) for j in range(1, n_tp)]
    for peer in peers:
        pl.semaphore_signal(barrier, inc=1, device_id=peer, device_id_type=MESH)
    loads = [
        pltpu.make_async_copy(src, dst, load_sem.at[n])
        for n, (src, dst) in enumerate(
            [(send_ref.at[e], full.at[0, m, t]), (wg_hbm, wg_ref), (wu_hbm, wu_ref), (wd_hbm, wd_ref)]
        )
    ]
    for load in loads:
        load.start()
    pl.semaphore_wait(barrier, len(peers))

    def remote(src, dst, kind, k, device):
        return pltpu.make_async_remote_copy(
            src_ref=src,
            dst_ref=dst,
            send_sem=send_sem.at[kind, k],
            recv_sem=recv_sem.at[kind, k],
            device_id=device,
            device_id_type=MESH,
        )

    def piece(k, src_m, src_t, cols=None):
        ref = full.at[k, src_m, src_t]
        return ref if cols is None else ref.at[:, cols]

    X, CORE_OWN, CORE_X = 0, 1, 2
    def y_kind(j): return 3 + (j - 1)
    def a_kind(j): return 3 + (n_tp - 1) + (j - 1)
    def b_kind(j): return 3 + 2 * (n_tp - 1) + (j - 1)
    def core_y(j): return 3 + 3 * (n_tp - 1) + (j - 1)
    def core_a(j): return 3 + 4 * (n_tp - 1) + (j - 1)
    def core_b(j): return 3 + 5 * (n_tp - 1) + (j - 1)
    Z = 3 + 6 * (n_tp - 1)

    def pass_on(ref, kind, k, device):
        remote(ref, ref, kind, k, device).start()

    def landed(ref, kind, k):
        remote(ref, ref, kind, k, (e, core_peer, t)).wait_recv()

    def sent(ref, kind, k):
        remote(ref, ref, kind, k, (e, core_peer, t)).wait_send()

    for k in range(1, experts):
        there = lax.rem(e + k, experts)
        remote(send_ref.at[there], full.at[k, m, t], Z, k, (there, m, t)).start()
    loads[0].wait()

    x_to, core_to = (e, x_peer, t), (e, core_peer, t)

    def own(k):
        mine = piece(k, m, t)
        @pl.when(k > 0)
        def _():
            landed(mine, Z, k)
        pass_on(mine, X, k, x_to)
        for j in range(1, n_tp):
            pass_on(mine, y_kind(j), k, (e, m, ahead(j)))
        pass_on(mine, CORE_OWN, k, core_to)

    def neighbours(k):
        across = piece(k, x_peer, t)
        landed(across, X, k)
        for j in range(1, n_tp):
            pass_on(piece(k, x_peer, t, last_cols), b_kind(j), k, (e, m, ahead(j)))
        pass_on(across, CORE_X, k, core_to)
        for j in range(1, n_tp):
            beside = piece(k, m, behind(j))
            landed(beside, y_kind(j), k)
            pass_on(piece(k, m, behind(j), first_cols), a_kind(j), k, x_to)
            pass_on(beside, core_y(j), k, core_to)

    def corners(k):
        for j in range(1, n_tp):
            for cols, kind, core in ((first_cols, a_kind, core_a), (last_cols, b_kind, core_b)):
                ref = piece(k, x_peer, behind(j), cols)
                landed(ref, kind(j), k)
                pass_on(ref, core(j), k, core_to)

    other_x = lax.rem(core_peer + 2, 4)

    def partner(k):
        landed(piece(k, core_peer, t), CORE_OWN, k)
        landed(piece(k, other_x, t), CORE_X, k)
        for j in range(1, n_tp):
            landed(piece(k, core_peer, behind(j)), core_y(j), k)
            landed(piece(k, other_x, behind(j), first_cols), core_a(j), k)
            landed(piece(k, other_x, behind(j), last_cols), core_b(j), k)
        pltpu.make_async_copy(full.at[k], x_hbm.at[k], out_sem.at[k]).start()

    def compute(k):
        def part(tp_at, base, size):
            return full[k, :, tp_at, :, base : base + size].reshape(held, size)

        def contract(base, w_ref, nt):
            total = None
            for tp_at in range(n_tp):
                cols = slice(tp_at * share, (tp_at + 1) * share)
                rows = part(tp_at, base, share)
                if nt:
                    term = lax.dot_general(rows, w_ref[0, :, cols], NT, preferred_element_type=F32)
                else:
                    term = jnp.dot(rows, w_ref[0, cols, :], preferred_element_type=F32)
                total = term if total is None else total + term
            return total

        gpre = contract(0, wg_ref, False)
        upre = contract(0, wu_ref, False)
        qvals = contract(share, wd_ref, True)
        extra = part(0, 2 * share, LANES).astype(F32)
        lane = lax.broadcasted_iota(jnp.int32, extra.shape, 1)
        weight = jnp.sum(jnp.where(lane == e, extra, 0.0), axis=1, keepdims=True)
        sig = jax.nn.sigmoid(gpre)
        silu_val = gpre * sig
        hidden = (silu_val * upre).astype(BF16).astype(F32)
        gate_part = jnp.sum(hidden * qvals, axis=1, keepdims=True)
        dhid = weight * qvals
        d_gate = (dhid * upre * sig * (1.0 + gpre * (1.0 - sig))).astype(BF16)
        d_up = (dhid * silu_val).astype(BF16)
        dg_ref[k] = d_gate
        du_ref[k] = d_up
        sc_ref[k] = (weight * hidden).astype(BF16)
        gate_lanes = jnp.where(lane == 0, gate_part, 0.0).astype(BF16)
        source = lax.rem(e + experts - k, experts)
        for tp_at in range(n_tp):
            cols = slice(tp_at * share, (tp_at + 1) * share)
            grad = lax.dot_general(d_gate, wg_ref[0, cols, :], NT, preferred_element_type=F32)
            grad = grad + lax.dot_general(d_up, wu_ref[0, cols, :], NT, preferred_element_type=F32)
            back_ref[:, tp_at, source, :, :share] = grad.astype(BF16).reshape(n_m, capacity, share)
            back_ref[:, tp_at, source, :, share:] = gate_lanes.reshape(n_m, capacity, LANES)

    def step(i, carry):
        pl.when(i < experts)(lambda: own(i))
        pl.when((i >= 1) & (i < experts + 1))(lambda: neighbours(i - 1))
        pl.when((i >= 2) & (i < experts + 2))(lambda: corners(i - 2))

        @pl.when(i == 3)
        def _():
            for load in loads[1:]:
                load.wait()

        @pl.when(i >= 3)
        def _():
            partner(i - 3)
            compute(i - 3)

        return carry

    lax.fori_loop(0, experts + 3, step, 0)

    def finish(k, carry):
        mine = piece(k, m, t)
        @pl.when(k > 0)
        def _():
            sent(mine, Z, k)
        sent(mine, X, k)
        sent(mine, CORE_OWN, k)
        sent(piece(k, x_peer, t), CORE_X, k)
        for j in range(1, n_tp):
            sent(mine, y_kind(j), k)
            sent(piece(k, x_peer, t, last_cols), b_kind(j), k)
            sent(piece(k, m, behind(j), first_cols), a_kind(j), k)
            sent(piece(k, m, behind(j)), core_y(j), k)
            sent(piece(k, x_peer, behind(j), first_cols), core_a(j), k)
            sent(piece(k, x_peer, behind(j), last_cols), core_b(j), k)
        pltpu.make_async_copy(full.at[k], x_hbm.at[k], out_sem.at[k]).wait()
        return carry

    lax.fori_loop(0, experts, finish, 0)


def grads_kernel(x_ref, c_ref, dg_ref, du_ref, sc_ref, gg_ref, gu_ref, gd_ref, sct):
    @pl.when(pl.program_id(0) == 0)
    def _():
        sct[...] = sc_ref[...].T

    tile = x_ref.shape[-1]
    rows = dg_ref.shape[0]
    xt = x_ref[:, :, 0].reshape(rows, tile).T
    gg_ref[0] = jnp.dot(xt, dg_ref[...], preferred_element_type=F32)
    gu_ref[0] = jnp.dot(xt, du_ref[...], preferred_element_type=F32)
    gd_ref[0] = jnp.dot(sct[...], c_ref[:, :, 0].reshape(rows, tile), preferred_element_type=F32)


def shards(tokens, routes, router_weight, gate_proj, up_proj, down_proj, cotangent):
    ntok, width = tokens.shape
    experts = router_weight.shape[1]
    n_m, n_tp = lax.axis_size("m"), lax.axis_size("tp")
    share = width // n_tp
    capacity = min(ntok, 5 * TOP * ntok // (4 * experts))
    capacity = -(-capacity // 16) * 16
    tp_index = lax.axis_index("tp")
    ff = gate_proj.shape[2]

    logits = jnp.dot(tokens, router_weight, preferred_element_type=F32)
    onehot = (routes[:, :, None] == jnp.arange(experts, dtype=jnp.int32)[None, None, :]).astype(F32)
    chosen = jnp.sum(onehot * logits[:, None, :], axis=2)
    first = jax.nn.sigmoid(chosen[:, 0] - chosen[:, 1])
    gates = jnp.stack([first, 1.0 - first], axis=1)
    used = gates.astype(BF16)
    named = jnp.sum(onehot, axis=1)
    below = (jnp.arange(ntok)[:, None] > jnp.arange(ntok)[None, :]).astype(BF16)
    rank = jnp.dot(below, named.astype(BF16), preferred_element_type=F32)
    slot = jnp.where(named > 0, rank, -1.0).astype(jnp.int32)
    place = (
        jnp.arange(capacity, dtype=jnp.int32)[None, :, None] == slot.T[:, None, :]
    ).astype(BF16)
    gate_cols = jnp.sum(onehot * used.astype(F32)[:, :, None], axis=1).astype(BF16)
    payload = jnp.concatenate(
        [
            lax.dynamic_slice_in_dim(tokens, tp_index * share, share, 1),
            lax.dynamic_slice_in_dim(cotangent, tp_index * share, share, 1),
            gate_cols,
            jnp.zeros((ntok, LANES - experts), BF16),
        ],
        axis=1,
    )
    rows = jnp.dot(
        place.reshape(experts * capacity, ntok), payload, preferred_element_type=F32
    ).astype(BF16)
    wide = 2 * share + LANES
    rows = rows.reshape(experts, capacity, wide)

    held = n_m * capacity
    back_wide = share + LANES
    hid_shape = jax.ShapeDtypeStruct((experts, held, ff), BF16)
    flops = 2 * experts * held * width * ff
    kinds = 4 + 6 * (n_tp - 1)
    vmem = pl.BlockSpec(memory_space=pltpu.VMEM)
    anywhere = pl.BlockSpec(memory_space=pl.ANY)
    full_shape = (experts, n_m, n_tp, capacity, wide)
    full, d_gate, d_up, scaled, back = pl.pallas_call(
        functools.partial(rows_kernel, share),
        in_specs=[vmem, anywhere, anywhere, anywhere],
        out_specs=[anywhere, vmem, vmem, vmem, vmem],
        out_shape=[
            jax.ShapeDtypeStruct(full_shape, BF16),
            hid_shape,
            hid_shape,
            hid_shape,
            jax.ShapeDtypeStruct((n_m, n_tp, experts, capacity, back_wide), BF16),
        ],
        scratch_shapes=[
            pltpu.VMEM(full_shape, BF16),
            pltpu.VMEM(gate_proj.shape, BF16),
            pltpu.VMEM(up_proj.shape, BF16),
            pltpu.VMEM(down_proj.shape, BF16),
            pltpu.SemaphoreType.DMA((experts,)),
            pltpu.SemaphoreType.DMA((kinds, experts)),
            pltpu.SemaphoreType.DMA((kinds, experts)),
            pltpu.SemaphoreType.DMA((4,)),
        ],
        compiler_params=pltpu.CompilerParams(
            collective_id=0, has_side_effects=True, vmem_limit_bytes=60 << 20
        ),
        cost_estimate=pl.CostEstimate(flops=5 * flops, bytes_accessed=30 << 20, transcendentals=0),
        name="rows",
    )(rows, gate_proj, up_proj, down_proj)

    mine = lax.psum_scatter(
        back.reshape(n_m * n_tp, experts * capacity, back_wide),
        ("m", "tp"),
        scatter_dimension=0,
        tiled=False,
    )

    tile = 256
    per = share // tile
    total = experts * held
    whole = lambda i: (0, 0)
    grad_gate, grad_up, grad_down = pl.pallas_call(
        grads_kernel,
        grid=(width // tile,),
        in_specs=[
            pl.BlockSpec((experts, n_m, 1, capacity, tile), lambda i: (0, 0, i // per, 0, i % per)),
            pl.BlockSpec((experts, n_m, 1, capacity, tile), lambda i: (0, 0, i // per, 0, per + i % per)),
            pl.BlockSpec((total, ff), whole),
            pl.BlockSpec((total, ff), whole),
            pl.BlockSpec((total, ff), whole),
        ],
        out_specs=[
            pl.BlockSpec((1, tile, ff), lambda i: (0, i, 0)),
            pl.BlockSpec((1, tile, ff), lambda i: (0, i, 0)),
            pl.BlockSpec((1, ff, tile), lambda i: (0, 0, i)),
        ],
        out_shape=[
            jax.ShapeDtypeStruct(gate_proj.shape, F32),
            jax.ShapeDtypeStruct(up_proj.shape, F32),
            jax.ShapeDtypeStruct(down_proj.shape, F32),
        ],
        scratch_shapes=[pltpu.VMEM((ff, total), BF16)],
        cost_estimate=pl.CostEstimate(flops=3 * flops, bytes_accessed=30 << 20, transcendentals=0),
        name="grads",
    )(full, full, d_gate.reshape(total, ff), d_up.reshape(total, ff), scaled.reshape(total, ff))

    home = lax.all_to_all(
        mine.reshape(experts, capacity, back_wide), "e", split_axis=0, concat_axis=0, tiled=True
    )
    route_sum = lax.dot_general(
        place.reshape(experts * capacity, ntok),
        home[:, :, :share].reshape(experts * capacity, share),
        (((0,), (0,)), ((), ())),
        preferred_element_type=F32,
    )
    gate_at = jnp.einsum(
        "ect,ecl->etl", place, home[:, :, share:], preferred_element_type=F32
    )[:, :, 0]
    gate_grad = jnp.sum(onehot * gate_at.T[:, None, :], axis=2)
    delta = first * (1.0 - first) * (gate_grad[:, 0] - gate_grad[:, 1])
    dlogits = delta[:, None] * (onehot[:, 0] - onehot[:, 1])
    router_rows = lax.dynamic_slice_in_dim(router_weight, tp_index * share, share, 0).astype(F32)
    router_part = lax.dot_general(dlogits, router_rows, NT, precision=lax.Precision.HIGHEST)
    token_grad = (route_sum + router_part).astype(BF16)
    n_ep = lax.axis_size("e") * n_m
    terms = lax.dot_general(
        dlogits, tokens.astype(F32), (((0,), (0,)), ((), ())), precision=lax.Precision.HIGHEST
    )
    terms = terms.reshape(experts, n_ep, width // n_ep).transpose(1, 0, 2)
    terms = lax.all_to_all(terms, ("e", "m"), split_axis=0, concat_axis=0, tiled=True)
    router_grad = jnp.sum(terms, axis=0).T
    return (token_grad, gate_grad, router_grad, grad_gate, grad_up, grad_down)


def solution(mesh):
    devices = mesh.devices
    grid = Mesh(
        devices.reshape(devices.shape[0] // MEMBERS, MEMBERS, devices.shape[1]), ("e", "m", "tp")
    )
    ep = ("e", "m")
    return jax.shard_map(
        shards,
        mesh=grid,
        in_specs=(
            P(ep, None),
            P(ep, None),
            P(),
            P(ep, None, "tp"),
            P(ep, None, "tp"),
            P(ep, "tp", None),
            P(ep, None),
        ),
        out_specs=(
            P(ep, "tp"),
            P(ep, None),
            P(ep, None),
            P(ep, None, "tp"),
            P(ep, None, "tp"),
            P(ep, "tp", None),
        ),
        check_vma=False,
    )
```

time: 265 us -> 196 us (0.74)
  waiting for transfers between devices: 195 us -> 74.9 us
  Pallas kernels: 34.9 us -> 87 us
  starting transfers between devices: 3.66 us -> 8.4 us
  matrix products: 9.57 us -> 5.82 us
    all_gather x2 -> x0, waiting for transfers between devices: 115 us -> none  [the longest x1 64.8 us: shards(): lax.all_gather(rows.reshape(held, wide), ('m', 'tp'), axis=0, tiled=False)]
    pallas_call x1, Pallas kernels: 20.2 us -> 72.4 us  [shards(): pl.pallas_call(functools.partial(rows_kernel, share), in_specs=[vmem, any...]
    reduce_scatter x2 -> x1, waiting for transfers between devices: 74.2 us -> 65.9 us  [shards(): lax.psum_scatter(back.reshape(n_m * n_tp, experts * capacity, back_wide),...]
    all_to_all x0 -> x1, starting transfers between devices: none -> 4.59 us  [shards(): lax.all_to_all(mine.reshape(experts, capacity, back_wide), 'e', split_axi...]
    all_to_all x0 -> x1, waiting for transfers between devices: none -> 3.92 us  [shards(): lax.all_to_all(mine.reshape(experts, capacity, back_wide), 'e', split_axi...]
    dot_general x2 -> x3, matrix products: 5.89 us -> 2.13 us  [the longest x1 1.6 us: shards(): jnp.dot(place.reshape(experts * capacity, ntok), payload, preferred_eleme...]
  transfers between devices with their start and end apart: 5 -> 3, of which waited for: 5 -> 3; matrix products, arithmetic and copies ran while one was open for 1% -> 1% of each run, Pallas kernels for 6% -> 8%
where the time goes in v2:
time: 196 us; the launch traced here: 195 us
  Pallas kernels  87 us (44%)
  waiting for transfers between devices  74.9 us (38%)
  between operations  14.2 us (7%)
  starting transfers between devices  8.4 us (4%)
  matrix products  5.82 us (3%)
  local copies, waits for them, and re-layouts  2.52 us (1%)
  other arithmetic  2.19 us (1%)
    pallas_call x1, Pallas kernels, shards(): pl.pallas_call(functools.partial(rows_kernel, share), in_specs=[vmem, any...  72.4 us
    reduce_scatter x1, waiting for transfers between devices, shards(): lax.psum_scatter(back.reshape(n_m * n_tp, experts * capacity, back_wide),...  65.9 us
    pallas_call x1, Pallas kernels, shards(): pl.pallas_call(grads_kernel, grid=(width // tile,), in_specs=[pl.BlockSpe...  14.7 us
    all_to_all x1, waiting for transfers between devices, shards(): lax.all_to_all(terms, ('e', 'm'), split_axis=0, concat_axis=0, tiled=True)  5.13 us
    all_to_all x1, starting transfers between devices, shards(): lax.all_to_all(mine.reshape(experts, capacity, back_wide), 'e', split_axi...  4.59 us
  transfers between devices with their start and end apart: 3, of which 3 were waited for; matrix products, arithmetic and copies ran while one was open for 1% of the time, Pallas kernels for 8%

profile of v2, /device:TPU:0, one launch (start us, length us, event | category | flops | bytes accessed | tf_op | source)
XLA Modules:
  0.0 195.1 jit_solution(17979137370902010011)
XLA Ops:
  7.2 0.7 copy-done
  7.9 1.3 fusion.19
  9.2 0.7 select_reduce_fusion.2
  9.9 0.1 eq.44
  10.0 0.7 select_reduce_fusion.1
  10.7 0.1 fusion.1
  10.8 0.1 copy.14
  11.0 0.1 bitcast_compare_fusion
  11.1 1.1 constant_dynamic-slice_fusion
  12.2 0.3 concatenate.8
  12.5 1.6 convolution_convert_fusion
  14.1 72.4 %rows.1 = (bf16[4,4,2,80,2176]{4,3,2,1,0:T(8,128)(2,1)}, bf16[4,320,512]{2,1,0:T(8,128)(2,1)}, bf16[4,320,512]{2,1,0:T(8,128)(2,1)}, bf16[4,320,512]{2,1,0:T(8,128)(2,1)}, bf16[4,2,4,80,1152]{4,3,2,1,0:T(8,128)(2,1)}) custom-call(bf16[4,80,2176]{2,1,0:T(8,128)(2,1)} %bitcast.37, bf16[1,2048,512]{2,1,0:T(8,128)(2,1)} %wg_hbm.1, bf16[1,2048,512]{2,1,0:T(8,128)(2,1)} %wu_hbm.1, ...), custom_call_target="tpu_custom_call" | custom-call | flops 13421772800 | bytes 31457280 | tf_op jit(solution)/shard_map/rows/pallas_call | solution.py:271
  86.5 65.9 %reduce-scatter.2.cloned.1.call-done = bf16[1,320,1152]{2,1,0:T(8,128)(2,1)} async-done(((bf16[8,320,1152]{2,1,0:T(8,128)(2,1)}), bf16[1,320,1152]{2,1,0:T(8,128)(2,1)}) %reduce-scatter.2.cloned.1.call-update) | async-done | bytes 737296 | tf_op jit(solution)/shard_map/reduce_scatter | solution.py:299
  152.4 4.6 %all-to-all-start = ((bf16[4,80,1152]{2,1,0:T(8,128)(2,1)}), bf16[4,80,1152]{2,1,0:T(8,128)(2,1)S(1)}, u32[]{:S(2)}, u32[]{:S(2)}) async-start(bf16[4,80,1152]{2,1,0:T(8,128)(2,1)} %bitcast.38), calls=%async_computation.1 | async-start | bytes 1474560 | tf_op jit(solution)/shard_map/all_to_all | solution.py:335
  157.0 0.3 copy.16
  157.3 14.7 %grads.1 = (f32[1,2048,512]{2,1,0:T(8,128)}, f32[1,2048,512]{2,1,0:T(8,128)}, f32[1,512,2048]{2,1,0:T(8,128)}) custom-call(bf16[4,4,2,80,2176]{4,3,2,1,0:T(8,128)(2,1)} %get-tuple-element.15.x_ref.c_ref, bf16[4,4,2,80,2176]{4,3,2,1,0:T(8,128)(2,1)} %get-tuple-element.15.x_ref.c_ref, bf16[1280,512]{1,0:T(8,128)(2,1)} %bitcast.41, bf16[1280,512]{1,0:T(8,128)(2,1)} %bitcast.42, ...), custom_call_target="tpu_custom_call" | custom-call | flops 8053063680 | bytes 31457280 | tf_op jit(solution)/shard_map/grads/pallas_call | solution.py:310
  171.9 3.9 %all-to-all-done = bf16[4,80,1152]{2,1,0:T(8,128)(2,1)S(1)} async-done(((bf16[4,80,1152]{2,1,0:T(8,128)(2,1)}), bf16[4,80,1152]{2,1,0:T(8,128)(2,1)S(1)}, u32[]{:S(2)}, u32[]{:S(2)}) %all-to-all-start) | async-done | bytes 737312 | tf_op jit(solution)/shard_map/all_to_all | solution.py:335
  175.9 0.2 fusion.3
  176.1 1.1 convolution_bitcast_fusion.1
  177.2 3.8 %all-to-all-start.1 = ((f32[16,4,128]{2,1,0:T(4,128)}), f32[16,4,128]{2,1,0:T(4,128)S(1)}, u32[]{:S(2)}, u32[]{:S(2)}) async-start(f32[16,4,128]{2,1,0:T(4,128)} %convolution_bitcast_fusion.1), calls=%async_computation.2 | async-start | bytes 65536 | tf_op jit(solution)/shard_map/all_to_all | solution.py:358
  181.0 0.3 convolution_bitcast_fusion
  181.3 1.2 fusion
  182.5 5.1 %all-to-all-done.1 = f32[16,4,128]{2,1,0:T(4,128)S(1)} async-done(((f32[16,4,128]{2,1,0:T(4,128)}), f32[16,4,128]{2,1,0:T(4,128)S(1)}, u32[]{:S(2)}, u32[]{:S(2)}) %all-to-all-start.1) | async-done | bytes 32800 | tf_op jit(solution)/shard_map/all_to_all | solution.py:358
  187.6 0.6 reduce_sum.49
  (17 shorter events, 0.2 us)
Async XLA Ops:
  7.2 0.7 copy-start
  7.2 145.2 %reduce-scatter.2.cloned.1.call-start = ((), (), s32[]{:S(2)}) async-start(), calls=%async_computation.3 | async-start | bytes 6635520 | tf_op jit(solution)/shard_map/reduce_scatter | solution.py:299
  86.5 70.5 %copy-start.1 = (bf16[128,2048]{1,0:T(8,128)(2,1)S(1)}, bf16[128,2048]{1,0:T(8,128)(2,1)}, u32[]{:S(2)}) copy-start(bf16[128,2048]{1,0:T(8,128)(2,1)} %param.7) | copy-start | bytes 1572868
  86.5 70.8 %copy-start.2 = (s32[128,2]{0,1:T(2,128)S(1)}, s32[128,2]{0,1:T(2,128)}, u32[]{:S(2)}) copy-start(s32[128,2]{0,1:T(2,128)} %param.8) | copy-start | bytes 3076
  152.4 23.5 %all-to-all-start = ((bf16[4,80,1152]{2,1,0:T(8,128)(2,1)}), bf16[4,80,1152]{2,1,0:T(8,128)(2,1)S(1)}, u32[]{:S(2)}, u32[]{:S(2)}) async-start(bf16[4,80,1152]{2,1,0:T(8,128)(2,1)} %bitcast.38), calls=%async_computation.1 | async-start | bytes 1474560 | tf_op jit(solution)/shard_map/all_to_all | solution.py:335
  176.1 12.2 %copy-start.3 = (f32[128,2]{0,1:T(2,128)}, f32[128,2]{0,1:T(2,128)S(1)}, u32[]{:S(2)}) copy-start(f32[128,2]{0,1:T(2,128)S(1)} %select_reduce_fusion) | copy-start | bytes 3076
  177.2 10.4 %all-to-all-start.1 = ((f32[16,4,128]{2,1,0:T(4,128)}), f32[16,4,128]{2,1,0:T(4,128)S(1)}, u32[]{:S(2)}, u32[]{:S(2)}) async-start(f32[16,4,128]{2,1,0:T(4,128)} %convolution_bitcast_fusion.1), calls=%async_computation.2 | async-start | bytes 65536 | tf_op jit(solution)/shard_map/all_to_all | solution.py:358
Sparse Core Ops, SparseCore 0:
  86.6 65.7 reduce-scatter.1
